TPU v7x, 32 devices: a whole 2x2x4 slice. The times are simulated.
32 devices in a mesh: sp: 8 (over z, x), tp: 4 (over y, core).
Axes of the slice: x: 2, y: 2, z: 4, core: 2. Of those that a mesh axis runs over, the one named last changes fastest.
Arguments:
- queries: bfloat16 [1024, 1024], P('sp', 'tp'), may hold values from -160 to 160
- keys: bfloat16 [1024, 256], P('sp', 'tp'), may hold values from -5 to 5
- values: bfloat16 [1024, 256], P('sp', 'tp'), may hold values from -6 to 6
- cum_gate: float32 [1024, 16], P('sp', 'tp'), as said below
- doc_ids: int32 [1024], P('sp'), may hold values from 0 to 7, never falling along the last dimension, each value on 1 to 640 neighbouring positions
- residual: bfloat16 [1024, 2048], P(('sp', 'tp')), may hold values from -6 to 6
- out_proj: bfloat16 [1024, 2048], replicated, may hold values from -0.1875 to 0.1875
- norm_gain: float32 [2048], replicated, may hold values from 0.1 to 1.9
- route_ids: int32 [1024, 2], P(('sp', 'tp')), may hold values from 0 to 7, all different within a row; in each aligned block of 32 rows (0 to 31, 32 to 63, ...) at most 16 rows name the same one
- route_weights: float32 [1024, 2], P(('sp', 'tp')), may hold values from 0.2 to 1
- expert_gate: bfloat16 [8, 2048, 1024], P('sp', None, 'tp'), may hold values from -0.125 to 0.125
- expert_up: bfloat16 [8, 2048, 1024], P('sp', None, 'tp'), may hold values from -0.125 to 0.125
- expert_down: bfloat16 [8, 1024, 2048], P('sp', 'tp'), may hold values from -0.1875 to 0.1875
Outputs:
- mixed: bfloat16 [1024, 2048], P(('sp', 'tp'))
Inputs may be any that keep to these rules, and one draw needn't show every extreme that they name: `route_ids`: within each aligned block of 32 rows no expert is named by more than 16 rows, and in every draw some block has an expert named by exactly 16 rows; the 2 experts of a row differ. `doc_ids`: never falling along positions; a document spans at most 640 positions, and one spans exactly that many. `cum_gate`: never rising along positions.
All inputs are finite; a program needn't handle non-finite values.
Results may differ from a plain program's by a relative error of at most 0.014.
Values may be sent and summed in bfloat16 or wider, within the bound.
A program may use at most 128 MiB of HBM per device.

v0:
```python
import jax
import jax.numpy as jnp
from jax import lax
from jax.sharding import PartitionSpec as P

D = 2048
HEAD_DIM = 64
TOP = 2


very_low = -1e30
norm_eps = 1e-06


def slot_ranks(picked_ids, experts):
    onehot = (picked_ids[..., None] == jnp.arange(experts, dtype=jnp.int32)).astype(jnp.int32)
    earlier = jnp.cumsum(onehot, axis=-2) - onehot
    return jnp.sum(earlier * onehot, axis=-1)


def local(
    queries,
    keys,
    values,
    cum_gate,
    doc_ids,
    residual,
    out_proj,
    norm_gain,
    route_ids,
    route_weights,
    expert_gate,
    expert_up,
    expert_down,
):
    own_tokens = queries.shape[0]
    head_count = queries.shape[1] // HEAD_DIM
    kv_count = keys.shape[1] // HEAD_DIM
    group_size = head_count // kv_count
    scale = HEAD_DIM ** (-0.5)
    own_start = lax.axis_index("sp") * own_tokens
    query_pos = own_start + jnp.arange(own_tokens, dtype=jnp.int32)
    query_heads = queries.reshape(own_tokens, kv_count, group_size, HEAD_DIM)
    query_gate = cum_gate.reshape(own_tokens, kv_count, group_size)
    gate_all, doc_all = (
        lax.all_gather(cum_gate, "sp", axis=0, tiled=True),
        lax.all_gather(doc_ids, "sp", axis=0, tiled=True),
    )

    def attend(state, key_block, value_block, first, block_len):
        gate_keys = lax.dynamic_slice_in_dim(gate_all, first, block_len, 0)
        doc_keys = lax.dynamic_slice_in_dim(doc_all, first, block_len, 0)
        key_heads = key_block.reshape(block_len, kv_count, HEAD_DIM)
        value_heads = value_block.reshape(block_len, kv_count, HEAD_DIM)
        scores = (
            jnp.einsum("tkgd,skd->tkgs", query_heads, key_heads, preferred_element_type=jnp.float32)
            * scale
        )
        scores = (
            scores
            + query_gate[..., None]
            - gate_keys.T.reshape(kv_count, group_size, block_len)[None]
        )
        key_pos = first + jnp.arange(block_len, dtype=jnp.int32)
        allowed = (key_pos[None, :] <= query_pos[:, None]) & (doc_keys[None, :] == doc_ids[:, None])
        allowed = allowed[:, None, None, :]
        scores = jnp.where(allowed, scores, very_low)
        top_old, total_old, summed_old = state
        top_new = jnp.maximum(top_old, jnp.max(scores, axis=-1))
        weights = jnp.where(allowed, jnp.exp(scores - top_new[..., None]), 0.0)
        fade = jnp.exp(top_old - top_new)
        total_new = total_old * fade + jnp.sum(weights, axis=-1)
        summed_new = summed_old * fade[..., None] + jnp.einsum(
            "tkgs,skd->tkgd",
            weights.astype(jnp.bfloat16),
            value_heads,
            preferred_element_type=jnp.float32,
        )
        return (top_new, total_new, summed_new)

    start_state = (
        jnp.full((own_tokens, kv_count, group_size), very_low, jnp.float32),
        jnp.zeros((own_tokens, kv_count, group_size), jnp.float32),
        jnp.zeros((own_tokens, kv_count, group_size, HEAD_DIM), jnp.float32),
    )
    key_piece = lax.all_gather(keys, "sp", axis=0, tiled=True)
    value_piece = lax.all_gather(values, "sp", axis=0, tiled=True)
    piece_len = key_piece.shape[0]
    block_len = min(piece_len, own_tokens)

    def one_block(index, inner):
        offset = index * block_len
        key_block = lax.dynamic_slice_in_dim(key_piece, offset, block_len, 0)
        value_block = lax.dynamic_slice_in_dim(value_piece, offset, block_len, 0)
        last_doc = lax.dynamic_index_in_dim(doc_all, offset + block_len - 1, 0, keepdims=False)
        needed = (offset <= own_start + own_tokens - 1) & (last_doc >= doc_ids[0])
        return lax.cond(
            needed,
            lambda carried: attend(carried, key_block, value_block, offset, block_len),
            lambda carried: carried,
            inner,
        )

    top, total, summed = lax.fori_loop(0, piece_len // block_len, one_block, start_state)
    attended = (
        (summed / total[..., None]).reshape(own_tokens, head_count * HEAD_DIM).astype(jnp.bfloat16)
    )
    sp_count = lax.axis_size("sp")
    rows_dev = residual.shape[0]
    plane_entries = lax.all_to_all(attended, "tp", split_axis=0, concat_axis=1, tiled=True)
    projected = jnp.dot(plane_entries, out_proj, preferred_element_type=jnp.float32)
    stream = (residual.astype(jnp.float32) + projected).astype(jnp.bfloat16)
    stream_f = stream.astype(jnp.float32)
    normed = stream_f * lax.rsqrt(jnp.mean(stream_f * stream_f, axis=1, keepdims=True) + norm_eps)
    normed = (normed * norm_gain[None, :]).astype(jnp.bfloat16)
    exp_dev = expert_gate.shape[0]
    experts = exp_dev * sp_count
    capacity = max(2, 2 * rows_dev * TOP // experts)
    own_flat = route_ids.reshape(-1)
    own_rank = slot_ranks(route_ids.reshape(1, rows_dev * TOP), experts)[0]
    own_dest = own_flat * capacity + own_rank
    row_of = jnp.arange(rows_dev * TOP, dtype=jnp.int32) // TOP
    outgoing = jnp.zeros((experts * capacity, D), jnp.bfloat16).at[own_dest].set(normed[row_of])
    arrived = lax.all_to_all(
        outgoing.reshape(experts, capacity, D), "sp", split_axis=0, concat_axis=1, tiled=True
    )
    arrived = arrived.reshape(exp_dev, sp_count, 1, capacity, D)
    piece = lax.all_gather(arrived, "tp", axis=2, tiled=True)
    gate = jnp.einsum("esncd,edf->esncf", piece, expert_gate, preferred_element_type=jnp.float32)
    upper = jnp.einsum("esncd,edf->esncf", piece, expert_up, preferred_element_type=jnp.float32)
    hidden = (jax.nn.silu(gate) * upper).astype(jnp.bfloat16)
    partial_value = jnp.einsum(
        "esncf,efd->esncd", hidden, expert_down, preferred_element_type=jnp.float32
    )
    expert_sums = lax.psum_scatter(
        partial_value.astype(jnp.bfloat16), "tp", scatter_dimension=2, tiled=True
    )
    expert_out = expert_sums.reshape(exp_dev, sp_count * capacity, D)
    returned = lax.all_to_all(expert_out, "sp", split_axis=1, concat_axis=0, tiled=True)
    selected = returned.reshape(experts * capacity, D)[own_dest]
    weighted = selected.astype(jnp.float32).reshape(rows_dev, TOP, D) * route_weights[..., None]
    return (stream_f + jnp.sum(weighted, axis=1)).astype(jnp.bfloat16)


def solution(mesh):
    in_specs = (
        P("sp", "tp"),
        P("sp", "tp"),
        P("sp", "tp"),
        P("sp", "tp"),
        P("sp"),
        P(("sp", "tp"), None),
        P(),
        P(),
        P(("sp", "tp"), None),
        P(("sp", "tp"), None),
        P("sp", None, "tp"),
        P("sp", None, "tp"),
        P("sp", "tp", None),
    )
    out_specs = P(("sp", "tp"), None)
    return jax.shard_map(local, mesh=mesh, in_specs=in_specs, out_specs=out_specs, check_vma=False)
```

profile of v0, /device:TPU:0, one launch (start us, length us, event | category | flops | bytes accessed | tf_op | source)
XLA Modules:
  0.0 276.8 jit_solution(1329913075445038006)
XLA Ops:
  6.5 28.3 %all_gather.16 = bf16[1024,64]{0,1:T(8,128)(2,1)S(1)} all-gather(bf16[128,64]{0,1:T(8,128)(2,1)} %param.18), channel_id=1, replica_groups=mesh['sp'=8,'tp'=4] {'sp'}, dimensions={0}, use_global_device_ids=true | all-gather | bytes 147456 | tf_op jit(solution)/shard_map/all_gather | solution.py:86
  34.8 26.4 %all_gather.18 = bf16[1024,64]{0,1:T(8,128)(2,1)S(1)} all-gather(bf16[128,64]{0,1:T(8,128)(2,1)} %param.19), channel_id=1, replica_groups=mesh['sp'=8,'tp'=4] {'sp'}, dimensions={0}, use_global_device_ids=true | all-gather | bytes 147456 | tf_op jit(solution)/shard_map/all_gather | solution.py:87
  61.2 0.9 copy.35
  62.2 26.3 %all_gather.17 = f32[1024,4]{0,1:T(4,128)S(1)} all-gather(f32[128,4]{0,1:T(4,128)} %param.20), channel_id=1, replica_groups=mesh['sp'=8,'tp'=4] {'sp'}, dimensions={0}, use_global_device_ids=true | all-gather | bytes 18432 | tf_op jit(solution)/shard_map/all_gather | solution.py:46
  88.4 16.5 %all-gather.1 = s32[8,1,128]{2,1,0:T(1,128)S(1)} all-gather(s32[1,1,128]{2,1,0:T(1,128)} %bitcast.128), channel_id=1, replica_groups=mesh['sp'=8,'tp'=4] {'sp'}, dimensions={0}, use_global_device_ids=true | all-gather | bytes 4608 | tf_op jit(solution)/shard_map/all_gather | solution.py:47
  105.0 18.1 %while.23 = (s32[]{:T(128)}, f32[128,1,4]{0,2,1:T(4,128)S(1)}, f32[128,1,4]{0,2,1:T(4,128)S(1)}, f32[128,1,4,64]{0,3,2,1:T(8,128)S(1)}, s32[]{:T(128)}, /*index=...) while((s32[]{:T(128)}, f32[128,1,4]{0,2,1:T(4,128)S(1)}, ...), condition=%wide.region_5.6_spmd.clone, body=%wide.region_0.5_spmd.clone.sunk | while | flops 17614608 | bytes 1258975 | solution.py:104
  105.0 0.7 dynamic_slice.68
  106.9 2.1 conditional.3
  107.1 0.8 compare_and_fusion
  107.8 0.9 fusion.47
  108.8 0.2 fusion.7
  109.1 0.7 dynamic_slice.68
  111.1 0.7 dynamic_slice.68
  113.1 0.7 dynamic_slice.68
  115.1 0.7 dynamic_slice.68
  117.1 0.7 dynamic_slice.68
  119.1 0.7 dynamic_slice.68
  121.1 0.7 dynamic_slice.68
  123.1 0.1 copy.36
  123.3 0.8 convert_element_type.76
  124.1 3.3 %all-to-all-start = ((bf16[4,32,256]{2,1,0:T(8,128)(2,1)}), bf16[4,32,256]{2,1,0:T(8,128)(2,1)S(1)}, u32[]{:S(2)}, u32[]{:S(2)}) async-start(bf16[4,32,256]{2,1,0:T(8,128)(2,1)} %convert_element_type.76), calls=%async_computation | async-start | bytes 131072 | tf_op jit(solution)/shard_map/all_to_all | solution.py:110
  127.5 0.1 eq.47
  127.7 0.1 reduce_window_sum.11
  127.8 0.2 select_reduce_fusion
  128.1 0.1 mul.107
  128.2 3.2 %all-to-all-done = bf16[4,32,256]{2,1,0:T(8,128)(2,1)S(1)} async-done(((bf16[4,32,256]{2,1,0:T(8,128)(2,1)}), bf16[4,32,256]{2,1,0:T(8,128)(2,1)S(1)}, u32[]{:S(2)}, u32[]{:S(2)}) %all-to-all-start) | async-done | bytes 65568 | tf_op jit(solution)/shard_map/all_to_all | solution.py:110
  131.5 3.1 %multiply_reduce_fusion.1 = (f32[32]{0:T(128)S(1)}, f32[32,2048]{1,0:T(8,128)S(1)}) fusion(bf16[32,1024]{1,0:T(8,128)(2,1)S(1)} %bitcast.124, bf16[1024,2048]{1,0:T(8,128)(2,1)} %param.23, bf16[32,2048]{1,0:T(8,128)(2,1)S(1)} %copy-done.1), kind=kOutput, calls=%fused_computation.58 | convolution fusion | flops 134610912 | bytes 4653184 | tf_op jit(solution)/shard_map/dot_general | solution.py:111
  134.7 2.0 scatter_custom_fusion
  136.7 22.0 %all_to_all.34 = bf16[8,16,2048]{2,1,0:T(8,128)(2,1)} all-to-all(bf16[8,16,2048]{2,1,0:T(8,128)(2,1)S(1)} %bitcast.121), channel_id=1, replica_groups=mesh['sp'=8,'tp'=4] {'sp'}, dimensions={0} | all-to-all | bytes 1048576 | tf_op jit(solution)/shard_map/all_to_all | solution.py:124
  158.8 20.8 %all-gather.4.cloned.1.call-done = bf16[8,64,2048]{2,1,0:T(8,128)(2,1)} async-done(((bf16[8,16,2048]{2,1,0:T(8,128)(2,1)}), bf16[8,64,2048]{2,1,0:T(8,128)(2,1)}) %all-gather.4.cloned.1.call-update) | async-done | bytes 2097168 | tf_op jit(solution)/shard_map/all_gather | solution.py:128
  179.6 2.3 fusion.30
  181.9 5.5 %fusion.24 = bf16[1,8,4,16,2048]{4,3,2,1,0:T(8,128)(2,1)} fusion(bf16[1,256,2048]{2,1,0:T(8,128)(2,1)S(1)} %copy-done, bf16[8,4,16,2048]{3,2,1,0:T(8,128)(2,1)} %bitcast.132, bf16[1,2048,256]{2,1,0:T(8,128)(2,1)} %param.28, f32[8,4,16,256]{3,2,1,0:T(8,128)S(1)} %fusion.30), kind=kOutput, calls=%fused_computation.36 | convolution fusion | flops 1075576832 | bytes 6815744 | tf_op jit(solution)/shard_map/esncf,efd->esncd/dot_general | solution.py:132
  187.4 0.6 copy-done.6
  188.0 0.6 dynamic-slice
  188.6 50.3 %all-reduce.3.cloned.1.call-done = bf16[1,8,4,16,2048]{4,3,2,1,0:T(8,128)(2,1)} async-done(((bf16[1,8,4,16,2048]{4,3,2,1,0:T(8,128)(2,1)}), bf16[1,8,4,16,2048]{4,3,2,1,0:T(8,128)(2,1)}) %all-reduce.3.cloned.1.call-update) | async-done | bytes 2097168
  238.9 1.7 constant_dynamic-slice_fusion
  240.6 0.8 copy.53
  241.5 0.5 broadcast.235
  242.0 3.7 %reduce.9 = bf16[128,2048]{1,0:T(8,128)(2,1)S(1)} reduce(bf16[128,1,2048]{2,1,0:T(2,128)(2,1)S(1)} %bitcast.119, bf16[]{:T(256)} %broadcast.235), dimensions={1}, to_apply=%bitcast.111.reduce_sub_computation | reduce | bytes 1048578
  245.7 1.2 reshape.400
  246.9 5.5 %all-to-all-start.2 = ((bf16[8,2,16384]{2,1,0:T(2,128)(2,1)}), bf16[8,2,16384]{2,1,0:T(2,128)(2,1)S(1)}, u32[]{:S(2)}, u32[]{:S(2)}) async-start(bf16[8,2,16384]{2,1,0:T(2,128)(2,1)} %reshape.400), calls=%async_computation.2 | async-start | bytes 1048576 | tf_op jit(solution)/shard_map/all_to_all | solution.py:139
  252.5 14.2 %all-to-all-done.2 = bf16[8,2,16384]{2,1,0:T(2,128)(2,1)S(1)} async-done(((bf16[8,2,16384]{2,1,0:T(2,128)(2,1)}), bf16[8,2,16384]{2,1,0:T(2,128)(2,1)S(1)}, u32[]{:S(2)}, u32[]{:S(2)}) %all-to-all-start.2) | async-done | bytes 524320 | tf_op jit(solution)/shard_map/all_to_all | solution.py:139
  266.6 0.5 reshape.401
  267.2 0.3 copy.52
  267.5 0.7 gather_fusion
  268.2 0.3 reshape.357
  268.6 0.7 multiply_reduce_fusion
  269.3 0.7 add_convert_fusion
  (55 shorter events, 1.0 us)
Async XLA Ops:
  6.5 175.3 %copy-start = (bf16[1,256,2048]{2,1,0:T(8,128)(2,1)S(1)}, bf16[1,256,2048]{2,1,0:T(8,128)(2,1)}, u32[]{:S(2)}) copy-start(bf16[1,256,2048]{2,1,0:T(8,128)(2,1)} %param.29) | copy-start | bytes 3145732
  104.9 22.5 %copy-start.3 = (s32[32,2]{0,1:T(2,128)S(1)}, s32[32,2]{0,1:T(2,128)}, u32[]{:S(2)}) copy-start(s32[32,2]{0,1:T(2,128)} %param.25) | copy-start | bytes 772
  105.0 26.5 %copy-start.1 = (bf16[32,2048]{1,0:T(8,128)(2,1)S(1)}, bf16[32,2048]{1,0:T(8,128)(2,1)}, u32[]{:S(2)}) copy-start(bf16[32,2048]{1,0:T(8,128)(2,1)} %param.22) | copy-start | bytes 393220
  124.1 7.4 %all-to-all-start = ((bf16[4,32,256]{2,1,0:T(8,128)(2,1)}), bf16[4,32,256]{2,1,0:T(8,128)(2,1)S(1)}, u32[]{:S(2)}, u32[]{:S(2)}) async-start(bf16[4,32,256]{2,1,0:T(8,128)(2,1)} %convert_element_type.76), calls=%async_computation | async-start | bytes 131072 | tf_op jit(solution)/shard_map/all_to_all | solution.py:110
  127.4 52.2 %all-gather.4.cloned.1.call-start = ((), (), s32[]{:S(2)}) async-start(), calls=%async_computation.3 | async-start | bytes 2621440 | tf_op jit(solution)/shard_map/all_gather | solution.py:128
  131.5 3.2 %copy-start.2 = (f32[2048]{0:T(1024)S(1)}, f32[2048]{0:T(1024)}, u32[]{:S(2)}) copy-start(f32[2048]{0:T(1024)} %param.24) | copy-start | bytes 24580
  134.6 45.0 %copy-start.5 = (bf16[1,2048,256]{2,1,0:T(8,128)(2,1)S(1)}, bf16[1,2048,256]{2,1,0:T(8,128)(2,1)}, u32[]{:S(2)}) copy-start(bf16[1,2048,256]{2,1,0:T(8,128)(2,1)} %param.27) | copy-start | bytes 3145732
  158.7 80.2 %all-reduce.3.cloned.1.call-start = ((), (), s32[]{:S(2)}) async-start(), calls=%async_computation.4 | async-start | bytes 4194304
  187.3 0.7 copy-start.6
  241.5 10.9 %copy-start.4 = (f32[32,2]{0,1:T(2,128)S(1)}, f32[32,2]{0,1:T(2,128)}, u32[]{:S(2)}) copy-start(f32[32,2]{0,1:T(2,128)} %param.26) | copy-start | bytes 772
  246.9 19.8 %all-to-all-start.2 = ((bf16[8,2,16384]{2,1,0:T(2,128)(2,1)}), bf16[8,2,16384]{2,1,0:T(2,128)(2,1)S(1)}, u32[]{:S(2)}, u32[]{:S(2)}) async-start(bf16[8,2,16384]{2,1,0:T(2,128)(2,1)} %reshape.400), calls=%async_computation.2 | async-start | bytes 1048576 | tf_op jit(solution)/shard_map/all_to_all | solution.py:139
Sparse Core Ops, SparseCore 0:
  158.8 20.6 all-gather.3
  187.5 51.3 all-reduce.2
where the time goes:
time: 280 us; the launch traced here: 277 us
  blocking collectives  119 us (42%)
  waiting for transfers between devices  88.5 us (32%)
  local copies, waits for them, and re-layouts  17 us (6%)
  between operations  13.7 us (5%)
  matrix products  12 us (4%)
  loops' own time  10.9 us (4%)
  starting transfers between devices  8.88 us (3%)
  other arithmetic  6.46 us (2%)
    unnamed x3, waiting for transfers between devices  50.4 us
    all_gather x1, blocking collectives, local(): key_piece = lax.all_gather(keys, 'sp', axis=0, tiled=True)  28.3 us
    all_gather x1, blocking collectives, local(): value_piece = lax.all_gather(values, 'sp', axis=0, tiled=True)  26.4 us
    all_gather x1, blocking collectives, local(): lax.all_gather(cum_gate, 'sp', axis=0, tiled=True)  26.3 us
    all_to_all x1, blocking collectives, local(): lax.all_to_all(outgoing.reshape(experts, capacity, D), 'sp', split_axis=0...  22 us
    all_gather x1, waiting for transfers between devices, local(): piece = lax.all_gather(arrived, 'tp', axis=2, tiled=True)  20.8 us
    all_gather x1, blocking collectives, local(): lax.all_gather(doc_ids, 'sp', axis=0, tiled=True)  16.5 us
    all_to_all x1, waiting for transfers between devices, local(): lax.all_to_all(expert_out, 'sp', split_axis=1, concat_axis=0, tiled=True)  14.2 us
  transfers between devices with their start and end apart: 4, of which 4 were waited for; matrix products, arithmetic and copies ran while one was open for 1% of the time, Pallas kernels for 0%

commit v1 on v0

--- a/solution.py
+++ b/solution.py
@@ -1,6 +1,10 @@
+import functools
+
 import jax
 import jax.numpy as jnp
 from jax import lax
+from jax.experimental import pallas as pl
+from jax.experimental.pallas import tpu as pltpu
 from jax.sharding import PartitionSpec as P
 
 D = 2048
@@ -142,6 +146,393 @@
     return (stream_f + jnp.sum(weighted, axis=1)).astype(jnp.bfloat16)
 
 
+def fused_kernel(
+    q, kv, aux, qaux, res, gain, idr, idc, wts, wo_hbm, wg_hbm, wu_hbm, wd_hbm,
+    out,
+    wo, wg, wu, wd, kvall, auxall, sc, mx, tot, acc, att, gath, proj, outg,
+    xin, p0, p1, p2, p3, r1, r3, ysum, ry, zsum, ret,
+    wsem, kv_s, kv_r, ax_s, ax_r, at_s, at_r, d_s, d_r, fy_s, fy_r, fp_s, fp_r, fq_s, fq_r,
+    c1_s, c1_r, c3_s, c3_r, cy_s, cy_r, cz_s, cz_r,
+    *, n_sp, n_tp, cap,
+):
+    me = lax.axis_index("sp")
+    t = lax.axis_index("tp")
+    tok, width = q.shape
+    heads = width // HEAD_DIM
+    rows = res.shape[0]
+    depth = res.shape[1]
+    slots = n_sp * cap
+    flip = lambda k: t + k - 2 * k * (lax.div(t, k) % 2)
+    partner = flip(1)
+    across = flip(2)
+    corner = 3 - t
+    f32, bf16 = jnp.float32, jnp.bfloat16
+
+    def remote(src, dst, ss, rs, dev):
+        return pltpu.make_async_remote_copy(
+            src_ref=src, dst_ref=dst, send_sem=ss, recv_sem=rs,
+            device_id=dev, device_id_type=pl.DeviceIdType.MESH,
+        )
+
+    def peer_at(k):
+        return lax.rem(me + k, n_sp)
+
+    loads = [
+        pltpu.make_async_copy(a, b, wsem.at[i])
+        for i, (a, b) in enumerate(((wo_hbm, wo), (wg_hbm, wg), (wu_hbm, wu), (wd_hbm, wd)))
+    ]
+    for c in loads:
+        c.start()
+
+    barrier = pltpu.get_barrier_semaphore()
+
+    def greet(k, _):
+        pl.semaphore_signal(barrier, inc=1, device_id=(peer_at(k), t), device_id_type=pl.DeviceIdType.MESH)
+        return 0
+
+    lax.fori_loop(1, n_sp, greet, 0)
+    for other in (partner, across, corner):
+        pl.semaphore_signal(barrier, inc=1, device_id=(me, other), device_id_type=pl.DeviceIdType.MESH)
+    pl.semaphore_wait(barrier, n_sp - 1 + n_tp - 1)
+
+    def kv_copies(dst_sp, src_sp):
+        return (
+            remote(kv, kvall.at[src_sp], kv_s.at[dst_sp], kv_r.at[src_sp], (dst_sp, t)),
+            remote(aux, auxall.at[src_sp], ax_s.at[dst_sp], ax_r.at[src_sp], (dst_sp, t)),
+        )
+
+    def send_kv(k, _):
+        for c in kv_copies(k, me):
+            c.start()
+        return 0
+
+    lax.fori_loop(me + 1, n_sp, send_kv, 0)
+    kvall[me] = kv[...]
+    auxall[me] = aux[...]
+
+    qpos = lax.broadcasted_iota(jnp.int32, (tok, tok), 0)
+    kpos = lax.broadcasted_iota(jnp.int32, (tok, tok), 1)
+    qdoc = qaux[:, heads : heads + 1]
+    scale = HEAD_DIM ** (-0.5)
+    for h in range(heads):
+        mx[h] = jnp.full((tok, tok), very_low, f32)
+        tot[h] = jnp.zeros((tok, tok), f32)
+        acc[h] = jnp.zeros((tok, 2 * HEAD_DIM), f32)
+
+    def first_pass(k, _):
+        j = me - k
+
+        @pl.when(k > 0)
+        def _():
+            for c in kv_copies(j, j):
+                c.wait_recv()
+
+        kb = kvall[j][:, :HEAD_DIM]
+        ax = auxall[j]
+        allowed = (kpos <= qpos + k * tok) & (ax[heads : heads + 1, :] == qdoc)
+        for h in range(heads):
+            s = lax.dot_general(
+                q[:, h * HEAD_DIM : (h + 1) * HEAD_DIM], kb, (((1,), (1,)), ((), ())),
+                preferred_element_type=f32,
+            )
+            s = s * scale + qaux[:, h : h + 1] - ax[h : h + 1, :]
+            s = jnp.where(allowed, s, very_low)
+            sc[j, h] = s
+            mx[h] = jnp.maximum(mx[h], s)
+        return 0
+
+    lax.fori_loop(0, me + 1, first_pass, 0)
+    for h in range(heads):
+        mx[h] = jnp.broadcast_to(jnp.max(mx[h], axis=1, keepdims=True), (tok, tok))
+
+    def second_pass(k, _):
+        j = me - k
+        vb = kvall[j]
+        for h in range(heads):
+            e = jnp.exp(sc[j, h] - mx[h])
+            tot[h] = tot[h] + e
+            acc[h] = acc[h] + jnp.dot(e.astype(bf16), vb, preferred_element_type=f32)
+        return 0
+
+    lax.fori_loop(0, me + 1, second_pass, 0)
+    pieces = [
+        (acc[h][:, HEAD_DIM:] / jnp.sum(tot[h], axis=1, keepdims=True)).astype(bf16)
+        for h in range(heads)
+    ]
+    att[...] = jnp.concatenate(pieces, axis=1)
+
+    def att_copy(to, frm):
+        return remote(
+            att.at[pl.ds(pl.multiple_of(to * rows, rows), rows), :], gath.at[frm],
+            at_s.at[to], at_r.at[frm], (me, to),
+        )
+
+    for other in (across, corner, partner):
+        att_copy(other, t).start()
+    gath[t] = att[pl.ds(pl.multiple_of(t * rows, rows), rows), :]
+
+    srow = lax.broadcasted_iota(jnp.int32, (slots, rows), 0)
+    scol = lax.broadcasted_iota(jnp.int32, (slots, rows), 1)
+    named = ((idr[0:1, :] == srow // cap) | (idr[1:2, :] == srow // cap)).astype(f32)
+    r_a = lax.broadcasted_iota(jnp.int32, (rows, rows), 0)
+    r_b = lax.broadcasted_iota(jnp.int32, (rows, rows), 1)
+    before = (r_a < r_b).astype(f32)
+    rank = jnp.dot(named.astype(bf16), before.astype(bf16), preferred_element_type=f32)
+    pick = jnp.where(rank == (srow % cap).astype(f32), named, 0.0).astype(bf16)
+    lane = lax.broadcasted_iota(jnp.int32, (rows, slots), 1)
+    back = [(idc[:, k : k + 1] == lane // cap).astype(f32) for k in range(TOP)]
+    after = (r_b < r_a).astype(bf16)
+    rank_t = jnp.dot(after, (back[0] + back[1]).astype(bf16), preferred_element_type=f32)
+    back = [jnp.where(rank_t == (lane % cap).astype(f32), b, 0.0).astype(bf16) for b in back]
+
+    loads[0].wait()
+    for i, src in enumerate((t, partner, across, corner)):
+        if i:
+            att_copy(src, src).wait_recv()
+        part = jnp.dot(
+            gath[src], wo[pl.ds(pl.multiple_of(src * width, width), width), :],
+            preferred_element_type=f32,
+        )
+        proj[...] = part if i == 0 else proj[...] + part
+    stream = (res[...].astype(f32) + proj[...]).astype(bf16)
+    stream_f = stream.astype(f32)
+    proj[...] = stream_f
+    normed = stream_f * lax.rsqrt(jnp.mean(stream_f * stream_f, axis=1, keepdims=True) + norm_eps)
+    normed = (normed * gain[...]).astype(bf16)
+    outg[...] = (
+        jnp.dot(pick, normed, preferred_element_type=f32).astype(bf16).reshape(n_sp, cap, depth)
+    )
+
+    def out_copy(to, frm):
+        return remote(outg.at[to], xin.at[t, frm], d_s.at[to], d_r.at[frm], (to, t))
+
+    def send_out(k, _):
+        out_copy(peer_at(k), me).start()
+        return 0
+
+    lax.fori_loop(1, n_sp, send_out, 0)
+    xin[t, me] = outg[me]
+
+    def to_across(j, line):
+        return remote(xin.at[line, j], xin.at[line, j], fy_s.at[j], fy_r.at[j], (me, across))
+
+    def to_partner(j, line):
+        return remote(xin.at[line, j], xin.at[line, j], fp_s.at[j], fp_r.at[j], (me, partner))
+
+    def relay_partner(j, line):
+        return remote(xin.at[line, j], xin.at[line, j], fq_s.at[j], fq_r.at[j], (me, partner))
+
+    def source_at(k):
+        return lax.rem(me - k + n_sp, n_sp)
+
+    def forward(k, _):
+        j = source_at(k)
+
+        @pl.when(k > 0)
+        def _():
+            out_copy(j, j).wait_recv()
+
+        to_across(j, t).start()
+        to_partner(j, t).start()
+
+        @pl.when(k > 0)
+        def _():
+            i = source_at(k - 1)
+            to_across(i, across).wait_recv()
+            relay_partner(i, across).start()
+
+        return 0
+
+    lax.fori_loop(0, n_sp, forward, 0)
+    last = source_at(n_sp - 1)
+    for c in loads[1:]:
+        c.wait()
+
+    def expert(line, dst):
+        x = xin[line].reshape(slots, depth)
+        g = jnp.dot(x, wg[...], preferred_element_type=f32)
+        u = jnp.dot(x, wu[...], preferred_element_type=f32)
+        hid = (g / (1.0 + jnp.exp(-g)) * u).astype(bf16)
+        dst[...] = (
+            jnp.dot(hid, wd[...], preferred_element_type=f32).astype(bf16).reshape(n_sp, cap, depth)
+        )
+
+    def all_of(fn):
+        def body(j, _):
+            fn(j)
+            return 0
+
+        lax.fori_loop(0, n_sp, body, 0)
+
+    expert(t, p0)
+    to_across(last, across).wait_recv()
+    relay_partner(last, across).start()
+    all_of(lambda j: to_partner(j, partner).wait_recv())
+    expert(partner, p1)
+
+    def c1_copy(j):
+        return remote(p1.at[j], r1.at[j], c1_s.at[j], c1_r.at[j], (me, partner))
+
+    def c3_copy(j):
+        return remote(p3.at[j], r3.at[j], c3_s.at[j], c3_r.at[j], (me, partner))
+
+    def cy_copy(j):
+        return remote(ysum.at[j], ry.at[j], cy_s.at[j], cy_r.at[j], (me, across))
+
+    def cz_copy(to, frm):
+        return remote(zsum.at[to], ret.at[frm], cz_s.at[to], cz_r.at[frm], (to, t))
+
+    all_of(lambda j: c1_copy(j).start())
+    expert(across, p2)
+    all_of(lambda j: relay_partner(j, corner).wait_recv())
+    expert(corner, p3)
+
+    def order(k):
+        return lax.rem(me + k, n_sp)
+
+    def start3(k, _):
+        c3_copy(order(k)).start()
+        return 0
+
+    lax.fori_loop(1, n_sp + 1, start3, 0)
+
+    def pair_sum(k, _):
+        j = order(k)
+        c3_copy(j).wait_recv()
+        ysum[j] = (p2[j].astype(f32) + r3[j].astype(f32)).astype(bf16)
+        cy_copy(j).start()
+        return 0
+
+    lax.fori_loop(1, n_sp + 1, pair_sum, 0)
+
+    def full_sum(k, _):
+        j = order(k)
+        c1_copy(j).wait_recv()
+        cy_copy(j).wait_recv()
+        zsum[j] = (p0[j].astype(f32) + r1[j].astype(f32) + ry[j].astype(f32)).astype(bf16)
+
+        @pl.when(k < n_sp)
+        def _():
+            cz_copy(j, me).start()
+
+        return 0
+
+    lax.fori_loop(1, n_sp + 1, full_sum, 0)
+    ret[me] = zsum[me]
+
+    def wait_ret(k, _):
+        j = source_at(k)
+        cz_copy(j, j).wait_recv()
+        return 0
+
+    lax.fori_loop(1, n_sp, wait_ret, 0)
+    total = proj[...]
+    got = ret[...].reshape(slots, depth)
+    mix = wts[:, 0:1] * jnp.dot(back[0], got, preferred_element_type=f32)
+    for k in range(1, TOP):
+        mix = mix + wts[:, k : k + 1] * jnp.dot(back[k], got, preferred_element_type=f32)
+    out[...] = (total + mix).astype(bf16)
+
+    def end_kv(k, _):
+        for c in kv_copies(k, me):
+            c.wait_send()
+        return 0
+
+    lax.fori_loop(me + 1, n_sp, end_kv, 0)
+    for other in (across, corner, partner):
+        att_copy(other, t).wait_send()
+
+    def end_peers(k, _):
+        j = peer_at(k)
+        out_copy(j, me).wait_send()
+        cz_copy(j, me).wait_send()
+        return 0
+
+    lax.fori_loop(1, n_sp, end_peers, 0)
+
+    def end_all(j):
+        to_across(j, t).wait_send()
+        to_partner(j, t).wait_send()
+        relay_partner(j, across).wait_send()
+        c1_copy(j).wait_send()
+        c3_copy(j).wait_send()
+        cy_copy(j).wait_send()
+
+    all_of(end_all)
+
+
+def fused(
+    queries, keys, values, cum_gate, doc_ids, residual, out_proj, norm_gain,
+    route_ids, route_weights, expert_gate, expert_up, expert_down,
+):
+    n_sp, n_tp = lax.axis_size("sp"), lax.axis_size("tp")
+    tok, width = queries.shape
+    heads = width // HEAD_DIM
+    rows, depth = residual.shape
+    cap = max(2, 2 * rows * TOP // n_sp)
+    ff = expert_gate.shape[2]
+    slots = n_sp * cap
+    f32, bf16 = jnp.float32, jnp.bfloat16
+    kv = jnp.concatenate([keys, values], axis=1)
+    qaux = jnp.concatenate([cum_gate, doc_ids.astype(f32)[:, None]], axis=1)
+    height = -(-(heads + 1) // 8) * 8
+    aux = jnp.pad(qaux.T, ((0, height - heads - 1), (0, 0)))
+    vm = pl.BlockSpec(memory_space=pltpu.VMEM)
+    hb = pl.BlockSpec(memory_space=pl.ANY)
+    block = pltpu.VMEM((n_sp, cap, depth), bf16)
+    dma = lambda n: pltpu.SemaphoreType.DMA((n,))
+    call = pl.pallas_call(
+        functools.partial(fused_kernel, n_sp=n_sp, n_tp=n_tp, cap=cap),
+        out_shape=jax.ShapeDtypeStruct((rows, depth), bf16),
+        in_specs=[vm] * 9 + [hb] * 4,
+        out_specs=vm,
+        scratch_shapes=[
+            pltpu.VMEM(out_proj.shape, bf16),
+            pltpu.VMEM((depth, ff), bf16),
+            pltpu.VMEM((depth, ff), bf16),
+            pltpu.VMEM((ff, depth), bf16),
+            pltpu.VMEM((n_sp, tok, 2 * HEAD_DIM), bf16),
+            pltpu.VMEM((n_sp, height, tok), f32),
+            pltpu.VMEM((n_sp, heads, tok, tok), f32),
+            pltpu.VMEM((heads, tok, tok), f32),
+            pltpu.VMEM((heads, tok, tok), f32),
+            pltpu.VMEM((heads, tok, 2 * HEAD_DIM), f32),
+            pltpu.VMEM((tok, width), bf16),
+            pltpu.VMEM((n_tp, rows, width), bf16),
+            pltpu.VMEM((rows, depth), f32),
+            block,
+            pltpu.VMEM((n_tp, n_sp, cap, depth), bf16),
+        ]
+        + [block] * 10
+        + [dma(4)]
+        + [dma(n_sp)] * 4
+        + [dma(n_tp)] * 2
+        + [dma(n_sp)] * 16,
+        compiler_params=pltpu.CompilerParams(
+            collective_id=0, has_side_effects=True, vmem_limit_bytes=60 * 1024 * 1024
+        ),
+    )
+    return call(
+        queries, kv, aux, qaux, residual, norm_gain.reshape(1, depth),
+        route_ids.T, route_ids, route_weights, out_proj, expert_gate[0], expert_up[0], expert_down[0],
+    )
+
+
+def chosen(*args):
+    n_sp, n_tp = lax.axis_size("sp"), lax.axis_size("tp")
+    queries, keys, residual, expert_gate = args[0], args[1], args[5], args[10]
+    cap = max(2, 2 * residual.shape[0] * TOP // n_sp)
+    fits = (
+        n_tp == 4
+        and expert_gate.shape[0] == 1
+        and keys.shape[1] == HEAD_DIM
+        and queries.shape[0] == 128
+        and cap % 16 == 0
+        and residual.shape[0] % 32 == 0
+    )
+    return fused(*args) if fits else local(*args)
+
+
 def solution(mesh):
     in_specs = (
         P("sp", "tp"),
@@ -159,4 +550,4 @@
         P("sp", "tp", None),
     )
     out_specs = P(("sp", "tp"), None)
-    return jax.shard_map(local, mesh=mesh, in_specs=in_specs, out_specs=out_specs, check_vma=False)
+    return jax.shard_map(chosen, mesh=mesh, in_specs=in_specs, out_specs=out_specs, check_vma=False)

time: 280 us -> 73.3 us (0.26)
  the two profiles are of different devices: /device:TPU:0 before, /device:TPU:11 now
where the time goes in v1:
time: 73.3 us; the launch traced here: 72.9 us
  Pallas kernels  63.6 us (87%)
  local copies, waits for them, and re-layouts  7.28 us (10%)
  other arithmetic  2.05 us (3%)
    pallas_call x1, Pallas kernels, fused(): call(queries, kv, aux, qaux, residual, norm_gain.reshape(1, depth), route...  63.6 us
    unnamed x5, local copies, waits for them, and re-layouts  5.95 us

profile of v1, /device:TPU:11, one launch (start us, length us, event | category | flops | bytes accessed | tf_op | source)
XLA Modules:
  0.0 72.9 jit_solution(12522837852507688272)
XLA Ops:
  0.0 0.7 convert_bitcast_fusion
  0.7 0.7 pad_maximum_fusion.1
  1.3 0.6 pad.4.aux
  1.9 1.4 %copy.25.wts = f32[32,2]{1,0:T(8,128)} copy(f32[32,2]{0,1:T(2,128)} %param.22) | data formatting | bytes 512 | tf_op args[9]
  3.3 1.4 %copy.24.idc = s32[32,2]{1,0:T(8,128)} copy(s32[32,2]{0,1:T(2,128)} %param.21) | data formatting | bytes 512 | tf_op args[8]
  4.7 0.8 %copy.21 = bf16[128,64]{1,0:T(8,128)(2,1)S(1)} copy(bf16[128,64]{0,1:T(8,128)(2,1)} %param.14) | data formatting | bytes 32768 | tf_op args[1]
  5.5 0.8 %copy.22 = bf16[128,64]{1,0:T(8,128)(2,1)S(1)} copy(bf16[128,64]{0,1:T(8,128)(2,1)} %param.15) | data formatting | bytes 32768 | tf_op args[2]
  6.3 0.7 pad_maximum_fusion.kv
  7.0 0.7 %copy.23.qaux = f32[128,5]{1,0:T(8,128)} copy(f32[128,5]{0,1:T(8,128)S(1)} %get-tuple-element.5) | data formatting | bytes 5120 | tf_op jit(solution)/shard_map/concatenate | solution.py:477
  7.8 63.6 %shard_map.127 = bf16[32,2048]{1,0:T(8,128)(2,1)} custom-call(bf16[128,256]{1,0:T(8,128)(2,1)} %q.1, bf16[128,128]{1,0:T(8,128)(2,1)} %pad_maximum_fusion.kv, f32[8,128]{1,0:T(8,128)} %pad.4.aux, f32[128,5]{1,0:T(8,128)} %copy.23.qaux, bf16[32,2048]{1,0:T(8,128)(2,1)} %res.1, f32[1,2048]{1,0:T(1,128)} %bitcast.12, s32[2,32]{1,0:T(2,128)} %bitcast.13, ...), custom_call_target="tpu_custom_call" | custom-call | tf_op jit(solution)/shard_map/pallas_call | solution.py:515
  71.4 1.6 %copy.27 = bf16[32,2048]{1,0:T(8,128)(2,1)} copy(bf16[32,2048]{1,0:T(8,128)(2,1)} %shard_map.127) | data formatting | bytes 262144

commit v2 on v0

--- a/solution.py
+++ b/solution.py
@@ -1,6 +1,10 @@
+import functools
+
 import jax
 import jax.numpy as jnp
 from jax import lax
+from jax.experimental import pallas as pl
+from jax.experimental.pallas import tpu as pltpu
 from jax.sharding import PartitionSpec as P
 
 D = 2048
@@ -142,6 +146,399 @@
     return (stream_f + jnp.sum(weighted, axis=1)).astype(jnp.bfloat16)
 
 
+def fused_kernel(
+    q, kt, vt, gt, doc, res, gain, idt, wtt, wo_hbm, wg_hbm, wu_hbm, wd_hbm,
+    base, mixed,
+    wo, wg, wu, wd, qs, kvall, auxall, sc, mx, tot, acc, att, gath, proj, outg,
+    xin, p0, p1, p2, p3, r1, r3, ysum, ry, zsum, ret,
+    wsem, kv_s, kv_r, ax_s, ax_r, kq_s, aq_s, at_s, at_r, d_s, d_r, fy_s, fy_r, fp_s, fp_r, fq_s, fq_r,
+    c1_s, c1_r, c3_s, c3_r, cy_s, cy_r, cz_s, cz_r,
+    *, n_sp, n_tp, cap,
+):
+    me = lax.axis_index("sp")
+    t = lax.axis_index("tp")
+    tok, width = q.shape
+    heads = width // HEAD_DIM
+    rows = res.shape[0]
+    depth = res.shape[1]
+    slots = n_sp * cap
+    half = n_sp // 2
+    flip = lambda k: t + k - 2 * k * (lax.div(t, k) % 2)
+    partner = flip(1)
+    across = flip(2)
+    corner = 3 - t
+    sib = me + 1 - 2 * lax.rem(me, 2)
+    f32, bf16 = jnp.float32, jnp.bfloat16
+
+    def remote(src, dst, ss, rs, dev):
+        return pltpu.make_async_remote_copy(
+            src_ref=src, dst_ref=dst, send_sem=ss, recv_sem=rs,
+            device_id=dev, device_id_type=pl.DeviceIdType.MESH,
+        )
+
+    def peer_at(k):
+        return lax.rem(me + k, n_sp)
+
+    def source_at(k):
+        return lax.rem(me - k + n_sp, n_sp)
+
+    def span(lo, hi, fn):
+        def body(k, _):
+            fn(k)
+            return 0
+
+        lax.fori_loop(lo, hi, body, 0)
+
+    loads = [
+        pltpu.make_async_copy(a, b, wsem.at[i])
+        for i, (a, b) in enumerate(((wo_hbm, wo), (wg_hbm, wg), (wu_hbm, wu), (wd_hbm, wd)))
+    ]
+    for c in loads:
+        c.start()
+    kvall[me, :HEAD_DIM, :] = kt[...]
+    kvall[me, HEAD_DIM:, :] = vt[...]
+    auxall[me, :heads, :] = gt[...]
+    auxall[me, heads : heads + 1, :] = doc[...].astype(f32)
+
+    barrier = pltpu.get_barrier_semaphore()
+    span(1, n_sp, lambda k: pl.semaphore_signal(
+        barrier, inc=1, device_id=(peer_at(k), t), device_id_type=pl.DeviceIdType.MESH))
+    for other in (partner, across, corner):
+        pl.semaphore_signal(barrier, inc=1, device_id=(me, other), device_id_type=pl.DeviceIdType.MESH)
+
+    def column(row, size):
+        eye = lax.broadcasted_iota(jnp.int32, (size, size), 0) == lax.broadcasted_iota(
+            jnp.int32, (size, size), 1
+        )
+        return jnp.sum(jnp.where(eye, jnp.broadcast_to(row, (size, size)), 0.0), axis=1, keepdims=True)
+
+    qpos = lax.broadcasted_iota(jnp.int32, (tok, tok), 0)
+    kpos = lax.broadcasted_iota(jnp.int32, (tok, tok), 1)
+    qdoc = column(doc[...].astype(f32), tok)
+    qgate = [column(gt[h : h + 1, :], tok) for h in range(heads)]
+    scale = HEAD_DIM ** (-0.5)
+    for h in range(heads):
+        qs[h] = q[:, h * HEAD_DIM : (h + 1) * HEAD_DIM]
+        mx[h] = jnp.full((tok, tok), very_low, f32)
+        tot[h] = jnp.zeros((tok, tok), f32)
+        acc[h] = jnp.zeros((tok, HEAD_DIM), f32)
+    pl.semaphore_wait(barrier, n_sp - 1 + n_tp - 1)
+    def kv_copies(to, frm):
+        return (
+            remote(kvall.at[frm], kvall.at[frm], kv_s.at[to], kv_r.at[frm], (to, t)),
+            remote(auxall.at[frm], auxall.at[frm], ax_s.at[to], ax_r.at[frm], (to, t)),
+        )
+
+    def kv_relays(frm):
+        return (
+            remote(kvall.at[frm], kvall.at[frm], kq_s.at[frm], kv_r.at[frm], (sib, t)),
+            remote(auxall.at[frm], auxall.at[frm], aq_s.at[frm], ax_r.at[frm], (sib, t)),
+        )
+
+    ahead = lax.div(n_sp - 1 - me, 2)
+
+    def kv_out(do):
+        def one(m):
+            for c in kv_copies(me + 2 * (ahead - m), me):
+                do(c)
+
+        span(0, ahead, one)
+
+        @pl.when(sib > me)
+        def _():
+            for c in kv_copies(sib, me):
+                do(c)
+
+    kv_out(lambda c: c.start())
+
+    def score_block(j):
+        kb = kvall[j, :HEAD_DIM, :]
+        ax = auxall[j]
+        allowed = (kpos + j * tok <= qpos + me * tok) & (ax[heads : heads + 1, :] == qdoc)
+        for h in range(heads):
+            s = jnp.dot(qs[h], kb, preferred_element_type=f32)
+            s = s * scale + qgate[h] - ax[h : h + 1, :]
+            s = jnp.where(allowed, s, very_low)
+            sc[j, h] = s
+            mx[h] = jnp.maximum(mx[h], s)
+
+    score_block(me)
+
+    def same_parity(m):
+        j = me - 2 * m
+        for c in kv_copies(j, j):
+            c.wait_recv()
+        for c in kv_relays(j):
+            c.start()
+        score_block(j)
+
+    span(1, lax.div(me, 2) + 1, same_parity)
+
+    def other_parity(m):
+        j = me - 1 - 2 * m
+        for c in kv_copies(j, j):
+            c.wait_recv()
+        score_block(j)
+
+    span(0, lax.div(me + 1, 2), other_parity)
+    for h in range(heads):
+        mx[h] = jnp.broadcast_to(jnp.max(mx[h], axis=1, keepdims=True), (tok, tok))
+
+    def second_pass(j):
+        vb = kvall[j, HEAD_DIM:, :]
+        for h in range(heads):
+            e = jnp.exp(sc[j, h] - mx[h])
+            tot[h] = tot[h] + e
+            acc[h] = acc[h] + lax.dot_general(
+                e.astype(bf16), vb, (((1,), (1,)), ((), ())), preferred_element_type=f32
+            )
+
+    span(0, me + 1, second_pass)
+    pieces = [
+        (acc[h] / jnp.sum(tot[h], axis=1, keepdims=True)).astype(bf16) for h in range(heads)
+    ]
+    att[...] = jnp.concatenate(pieces, axis=1)
+    def att_copy(to, frm):
+        return remote(
+            att.at[pl.ds(pl.multiple_of(to * rows, rows), rows), :], gath.at[frm],
+            at_s.at[to], at_r.at[frm], (me, to),
+        )
+
+    for other in (across, corner, partner):
+        att_copy(other, t).start()
+    gath[t] = att[pl.ds(pl.multiple_of(t * rows, rows), rows), :]
+
+    srow = lax.broadcasted_iota(jnp.int32, (slots, rows), 0)
+    named = ((idt[0:1, :] == srow // cap) | (idt[1:2, :] == srow // cap)).astype(f32)
+    r_a = lax.broadcasted_iota(jnp.int32, (rows, rows), 0)
+    r_b = lax.broadcasted_iota(jnp.int32, (rows, rows), 1)
+    before = (r_a < r_b).astype(bf16)
+    rank = jnp.dot(named.astype(bf16), before, preferred_element_type=f32)
+    pick = jnp.where(rank == (srow % cap).astype(f32), named, 0.0).astype(bf16)
+    lane = lax.broadcasted_iota(jnp.int32, (rows, slots), 1)
+    owner = (lane // cap).astype(f32)
+    back = [(column(idt[k : k + 1, :].astype(f32), rows) == owner).astype(f32) for k in range(TOP)]
+    share = [column(wtt[k : k + 1, :], rows) for k in range(TOP)]
+    after = (r_b < r_a).astype(bf16)
+    rank_t = jnp.dot(after, (back[0] + back[1]).astype(bf16), preferred_element_type=f32)
+    back = [jnp.where(rank_t == (lane % cap).astype(f32), b, 0.0).astype(bf16) for b in back]
+    loads[0].wait()
+    for i, src in enumerate((t, partner, across, corner)):
+        if i:
+            att_copy(src, src).wait_recv()
+        part = jnp.dot(
+            gath[src], wo[pl.ds(pl.multiple_of(src * width, width), width), :],
+            preferred_element_type=f32,
+        )
+        proj[...] = part if i == 0 else proj[...] + part
+    stream = (res[...].astype(f32) + proj[...]).astype(bf16)
+    base[...] = stream
+    stream_f = stream.astype(f32)
+    normed = stream_f * lax.rsqrt(jnp.mean(stream_f * stream_f, axis=1, keepdims=True) + norm_eps)
+    normed = (normed * gain[...]).astype(bf16)
+    outg[...] = (
+        jnp.dot(pick, normed, preferred_element_type=f32).astype(bf16).reshape(n_sp, cap, depth)
+    )
+    def out_copy(k):
+        to = peer_at(k)
+        return remote(outg.at[to], xin.at[t, k], d_s.at[k], d_r.at[k], (to, t))
+
+    def to_across(k, line):
+        return remote(xin.at[line, k], xin.at[line, k], fy_s.at[k], fy_r.at[k], (me, across))
+
+    def to_partner(k, line):
+        return remote(xin.at[line, k], xin.at[line, k], fp_s.at[k], fp_r.at[k], (me, partner))
+
+    def relay_partner(k, line):
+        return remote(xin.at[line, k], xin.at[line, k], fq_s.at[k], fq_r.at[k], (me, partner))
+
+    def c1_copy(k):
+        return remote(p1.at[k], r1.at[k], c1_s.at[k], c1_r.at[k], (me, partner))
+
+    def c3_copy(k):
+        return remote(p3.at[k], r3.at[k], c3_s.at[k], c3_r.at[k], (me, partner))
+
+    def cy_copy(k):
+        return remote(ysum.at[k], ry.at[k], cy_s.at[k], cy_r.at[k], (me, across))
+
+    def cz_copy(k, frm):
+        return remote(zsum.at[k], ret.at[frm], cz_s.at[k], cz_r.at[k], (source_at(k), t))
+
+    span(1, n_sp, lambda k: out_copy(k).start())
+    xin[t, 0] = outg[me]
+    to_across(0, t).start()
+    to_partner(0, t).start()
+
+    def relay(k):
+        to_across(k, across).wait_recv()
+        relay_partner(k, across).start()
+
+    def forward(k):
+        out_copy(k).wait_recv()
+        to_across(k, t).start()
+        to_partner(k, t).start()
+        relay(k - 1)
+
+    def expert(line, lo, dst):
+        x = xin[line, lo : lo + half].reshape(half * cap, depth)
+        g = jnp.dot(x, wg[...], preferred_element_type=f32)
+        u = jnp.dot(x, wu[...], preferred_element_type=f32)
+        hid = (g / (1.0 + jnp.exp(-g)) * u).astype(bf16)
+        dst[lo : lo + half] = (
+            jnp.dot(hid, wd[...], preferred_element_type=f32).astype(bf16).reshape(half, cap, depth)
+        )
+
+    def pair_sum(k):
+        c3_copy(k).wait_recv()
+        ysum[k] = (p2[k].astype(f32) + r3[k].astype(f32)).astype(bf16)
+        cy_copy(k).start()
+
+    def full_sum(k):
+        c1_copy(k).wait_recv()
+        cy_copy(k).wait_recv()
+        zsum[k] = (p0[k].astype(f32) + r1[k].astype(f32) + ry[k].astype(f32)).astype(bf16)
+
+        @pl.when(k > 0)
+        def _():
+            cz_copy(k, me).start()
+
+    span(1, half + 1, forward)
+    for c in loads[1:]:
+        c.wait()
+    expert(t, 0, p0)
+    span(half + 1, half + 2, forward)
+    span(0, half, lambda k: to_partner(k, partner).wait_recv())
+    expert(partner, 0, p1)
+    span(0, half, lambda k: c1_copy(k).start())
+    span(half + 2, n_sp - 1, forward)
+    span(0, half, lambda k: relay_partner(k, corner).wait_recv())
+    expert(corner, 0, p3)
+    span(0, half, lambda k: c3_copy(k).start())
+    span(n_sp - 1, n_sp, forward)
+    expert(across, 0, p2)
+    span(0, half, pair_sum)
+    expert(t, half, p0)
+    relay(n_sp - 1)
+    span(half, n_sp, lambda k: to_partner(k, partner).wait_recv())
+    expert(partner, half, p1)
+    span(half, n_sp, lambda k: c1_copy(k).start())
+    span(half, n_sp, lambda k: relay_partner(k, corner).wait_recv())
+    expert(corner, half, p3)
+    span(half, n_sp, lambda k: c3_copy(k).start())
+    expert(across, half, p2)
+    span(half, n_sp, pair_sum)
+    span(0, half, full_sum)
+    span(half, n_sp, full_sum)
+    ret[me] = zsum[0]
+    span(1, n_sp, lambda k: cz_copy(k, peer_at(k)).wait_recv())
+    got = ret[...].reshape(slots, depth)
+    mix = share[0] * jnp.dot(back[0], got, preferred_element_type=f32)
+    for k in range(1, TOP):
+        mix = mix + share[k] * jnp.dot(back[k], got, preferred_element_type=f32)
+    mixed[...] = mix
+    kv_out(lambda c: c.wait_send())
+
+    def end_relay(m):
+        for c in kv_relays(me - 2 * m):
+            c.wait_send()
+
+    span(1, lax.div(me, 2) + 1, end_relay)
+    for other in (across, corner, partner):
+        att_copy(other, t).wait_send()
+
+    def end_peers(k):
+        out_copy(k).wait_send()
+        cz_copy(k, me).wait_send()
+
+    span(1, n_sp, end_peers)
+
+    def end_all(k):
+        to_across(k, t).wait_send()
+        to_partner(k, t).wait_send()
+        relay_partner(k, across).wait_send()
+        c1_copy(k).wait_send()
+        c3_copy(k).wait_send()
+        cy_copy(k).wait_send()
+
+    span(0, n_sp, end_all)
+
+
+def fused(
+    queries, keys, values, cum_gate, doc_ids, residual, out_proj, norm_gain,
+    route_ids, route_weights, expert_gate, expert_up, expert_down,
+):
+    n_sp, n_tp = lax.axis_size("sp"), lax.axis_size("tp")
+    tok, width = queries.shape
+    heads = width // HEAD_DIM
+    rows, depth = residual.shape
+    cap = max(2, 2 * rows * TOP // n_sp)
+    ff = expert_gate.shape[2]
+    slots = n_sp * cap
+    f32, bf16 = jnp.float32, jnp.bfloat16
+    height = -(-(heads + 1) // 8) * 8
+    vm = pl.BlockSpec(memory_space=pltpu.VMEM)
+    hb = pl.BlockSpec(memory_space=pl.ANY)
+    block = pltpu.VMEM((n_sp, cap, depth), bf16)
+    dma = lambda n: pltpu.SemaphoreType.DMA((n,))
+    call = pl.pallas_call(
+        functools.partial(fused_kernel, n_sp=n_sp, n_tp=n_tp, cap=cap),
+        out_shape=(
+            jax.ShapeDtypeStruct((rows, depth), bf16),
+            jax.ShapeDtypeStruct((rows, depth), f32),
+        ),
+        in_specs=[vm] * 9 + [hb] * 4,
+        out_specs=(vm, vm),
+        scratch_shapes=[
+            pltpu.VMEM(out_proj.shape, bf16),
+            pltpu.VMEM((depth, ff), bf16),
+            pltpu.VMEM((depth, ff), bf16),
+            pltpu.VMEM((ff, depth), bf16),
+            pltpu.VMEM((heads, tok, HEAD_DIM), bf16),
+            pltpu.VMEM((n_sp, 2 * HEAD_DIM, tok), bf16),
+            pltpu.VMEM((n_sp, height, tok), f32),
+            pltpu.VMEM((n_sp, heads, tok, tok), f32),
+            pltpu.VMEM((heads, tok, tok), f32),
+            pltpu.VMEM((heads, tok, tok), f32),
+            pltpu.VMEM((heads, tok, HEAD_DIM), f32),
+            pltpu.VMEM((tok, width), bf16),
+            pltpu.VMEM((n_tp, rows, width), bf16),
+            pltpu.VMEM((rows, depth), f32),
+            block,
+            pltpu.VMEM((n_tp, n_sp, cap, depth), bf16),
+        ]
+        + [block] * 10
+        + [dma(4)]
+        + [dma(n_sp)] * 6
+        + [dma(n_tp)] * 2
+        + [dma(n_sp)] * 16,
+        compiler_params=pltpu.CompilerParams(
+            collective_id=0, has_side_effects=True, vmem_limit_bytes=60 * 1024 * 1024
+        ),
+    )
+    base, mixed = call(
+        queries, keys.T, values.T, cum_gate.T, doc_ids.reshape(1, tok), residual, norm_gain.reshape(1, depth),
+        route_ids.T, route_weights.T, out_proj, expert_gate[0], expert_up[0], expert_down[0],
+    )
+    return (base.astype(f32) + mixed).astype(bf16)
+
+
+def chosen(*args):
+    n_sp, n_tp = lax.axis_size("sp"), lax.axis_size("tp")
+    queries, keys, residual, expert_gate = args[0], args[1], args[5], args[10]
+    cap = max(2, 2 * residual.shape[0] * TOP // n_sp)
+    fits = (
+        n_tp == 4
+        and n_sp % 2 == 0
+        and n_sp >= 8
+        and expert_gate.shape[0] == 1
+        and keys.shape[1] == HEAD_DIM
+        and queries.shape[0] == 128
+        and cap % 16 == 0
+        and residual.shape[0] % 32 == 0
+    )
+    return fused(*args) if fits else local(*args)
+
+
 def solution(mesh):
     in_specs = (
         P("sp", "tp"),
@@ -159,4 +556,4 @@
         P("sp", "tp", None),
     )
     out_specs = P(("sp", "tp"), None)
-    return jax.shard_map(local, mesh=mesh, in_specs=in_specs, out_specs=out_specs, check_vma=False)
+    return jax.shard_map(chosen, mesh=mesh, in_specs=in_specs, out_specs=out_specs, check_vma=False)

time: 280 us -> 64.3 us (0.23); the launches traced: 277 us -> 64.2 us
  blocking collectives: 119 us -> 0 us
  waiting for transfers between devices: 88.5 us -> 0 us
  Pallas kernels: 0 us -> 62.5 us
  local copies, waits for them, and re-layouts: 17 us -> 0 us
  between operations: 13.7 us -> 0.01 us
  matrix products: 12 us -> 0 us
  loops' own time: 10.9 us -> 0 us
  starting transfers between devices: 8.88 us -> 0 us
  other arithmetic: 6.46 us -> 1.66 us
    all_gather x4 -> x0, blocking collectives: 97.4 us -> none  [the longest x1 28.3 us: local(): key_piece = lax.all_gather(keys, 'sp', axis=0, tiled=True)]
    pallas_call x0 -> x1, Pallas kernels: none -> 62.5 us  [fused(): call(queries, keys.T, values.T, cum_gate.T, doc_ids.reshape(1, tok), resi...]
    unnamed x3 -> x0, waiting for transfers between devices: 50.4 us -> none
    all_to_all x1 -> x0, blocking collectives: 22 us -> none  [local(): lax.all_to_all(outgoing.reshape(experts, capacity, D), 'sp', split_axis=0...]
    all_gather x1 -> x0, waiting for transfers between devices: 20.8 us -> none  [local(): piece = lax.all_gather(arrived, 'tp', axis=2, tiled=True)]
    all_to_all x2 -> x0, waiting for transfers between devices: 17.4 us -> none  [the longest x1 14.2 us: local(): lax.all_to_all(expert_out, 'sp', split_axis=1, concat_axis=0, tiled=True)]
    dot_general x5 -> x0, matrix products: 12 us -> none  [the longest x1 5.46 us: local(): jnp.einsum('esncf,efd->esncd', hidden, expert_down, preferred_element_typ...]
    another operation x9 -> x0, loops' own time: 10.9 us -> none  [the longest x1 10.7 us: local(): lax.fori_loop(0, piece_len // block_len, one_block, start_state)]
  transfers between devices with their start and end apart: 4 -> 0, of which waited for: 4 -> 0; matrix products, arithmetic and copies ran while one was open for 1% -> 0% of each run, Pallas kernels for 0% -> 0%
where the time goes in v2:
time: 64.3 us; the launch traced here: 64.2 us
  Pallas kernels  62.5 us (97%)
  other arithmetic  1.66 us (3%)
    pallas_call x1, Pallas kernels, fused(): call(queries, keys.T, values.T, cum_gate.T, doc_ids.reshape(1, tok), resi...  62.5 us
    convert_element_type x1, other arithmetic, fused(): return (base.astype(f32) + mixed).astype(bf16)  1.66 us

profile of v2, /device:TPU:0, one launch (start us, length us, event | category | flops | bytes accessed | tf_op | source)
XLA Modules:
  0.0 64.2 jit_solution(12891655069984258447)
XLA Ops:
  0.0 62.5 %shard_map.127 = (bf16[32,2048]{1,0:T(8,128)(2,1)}, f32[32,2048]{1,0:T(8,128)}) custom-call(bf16[128,256]{1,0:T(8,128)(2,1)} %q.1, bf16[64,128]{1,0:T(8,128)(2,1)} %bitcast.13, bf16[64,128]{1,0:T(8,128)(2,1)} %bitcast.14, f32[4,128]{1,0:T(4,128)} %bitcast.16, s32[1,128]{1,0:T(1,128)} %bitcast.19, bf16[32,2048]{1,0:T(8,128)(2,1)} %res.1, f32[1,2048]{1,0:T(1,128)} %bitcast.15, ...), custom_call_target="tpu_custom_call" | custom-call | tf_op jit(solution)/shard_map/pallas_call | solution.py:518
  62.5 1.7 %add_convert_fusion = bf16[32,2048]{1,0:T(8,128)(2,1)} fusion(f32[32,2048]{1,0:T(8,128)} %get-tuple-element.8, bf16[32,2048]{1,0:T(8,128)(2,1)} %get-tuple-element.7), kind=kLoop, calls=%fused_computation | loop fusion | flops 196608 | bytes 524288 | tf_op jit(solution)/shard_map/convert_element_type | solution.py:522

commit v3 on v2

--- a/solution.py
+++ b/solution.py
@@ -150,7 +150,7 @@
     q, kt, vt, gt, doc, res, gain, idt, wtt, wo_hbm, wg_hbm, wu_hbm, wd_hbm,
     base, mixed,
     wo, wg, wu, wd, qs, kvall, auxall, sc, mx, tot, acc, att, gath, proj, outg,
-    xin, p0, p1, p2, p3, r1, r3, ysum, ry, zsum, ret,
+    xin, pc, r1, r3, ysum, ry, zsum, ret,
     wsem, kv_s, kv_r, ax_s, ax_r, kq_s, aq_s, at_s, at_r, d_s, d_r, fy_s, fy_r, fp_s, fp_r, fq_s, fq_r,
     c1_s, c1_r, c3_s, c3_r, cy_s, cy_r, cz_s, cz_r,
     *, n_sp, n_tp, cap,
@@ -162,7 +162,7 @@
     rows = res.shape[0]
     depth = res.shape[1]
     slots = n_sp * cap
-    half = n_sp // 2
+    part = n_sp // 4
     flip = lambda k: t + k - 2 * k * (lax.div(t, k) % 2)
     partner = flip(1)
     across = flip(2)
@@ -179,8 +179,17 @@
     def peer_at(k):
         return lax.rem(me + k, n_sp)
 
-    def source_at(k):
-        return lax.rem(me - k + n_sp, n_sp)
+    def swap_at(k):
+        bits, at = [], 1
+        while at < n_sp:
+            bits.append((lax.rem(lax.div(k, at), 2), lax.rem(lax.div(me, at), 2), at))
+            at *= 2
+        want = [b[0] for b in bits]
+        want[1], want[2] = want[2], want[1] + want[2] - 2 * want[1] * want[2]
+        j = me
+        for w, (_, m, p) in zip(want, bits):
+            j = j + (w - 2 * w * m) * p
+        return j
 
     def span(lo, hi, fn):
         def body(k, _):
@@ -326,11 +335,11 @@
     for i, src in enumerate((t, partner, across, corner)):
         if i:
             att_copy(src, src).wait_recv()
-        part = jnp.dot(
+        term = jnp.dot(
             gath[src], wo[pl.ds(pl.multiple_of(src * width, width), width), :],
             preferred_element_type=f32,
         )
-        proj[...] = part if i == 0 else proj[...] + part
+        proj[...] = term if i == 0 else proj[...] + term
     stream = (res[...].astype(f32) + proj[...]).astype(bf16)
     base[...] = stream
     stream_f = stream.astype(f32)
@@ -340,7 +349,7 @@
         jnp.dot(pick, normed, preferred_element_type=f32).astype(bf16).reshape(n_sp, cap, depth)
     )
     def out_copy(k):
-        to = peer_at(k)
+        to = swap_at(k)
         return remote(outg.at[to], xin.at[t, k], d_s.at[k], d_r.at[k], (to, t))
 
     def to_across(k, line):
@@ -353,16 +362,16 @@
         return remote(xin.at[line, k], xin.at[line, k], fq_s.at[k], fq_r.at[k], (me, partner))
 
     def c1_copy(k):
-        return remote(p1.at[k], r1.at[k], c1_s.at[k], c1_r.at[k], (me, partner))
+        return remote(pc.at[partner, k], r1.at[k], c1_s.at[k], c1_r.at[k], (me, partner))
 
     def c3_copy(k):
-        return remote(p3.at[k], r3.at[k], c3_s.at[k], c3_r.at[k], (me, partner))
+        return remote(pc.at[corner, k], r3.at[k], c3_s.at[k], c3_r.at[k], (me, partner))
 
     def cy_copy(k):
         return remote(ysum.at[k], ry.at[k], cy_s.at[k], cy_r.at[k], (me, across))
 
     def cz_copy(k, frm):
-        return remote(zsum.at[k], ret.at[frm], cz_s.at[k], cz_r.at[k], (source_at(k), t))
+        return remote(zsum.at[k], ret.at[frm], cz_s.at[k], cz_r.at[k], (swap_at(k), t))
 
     span(1, n_sp, lambda k: out_copy(k).start())
     xin[t, 0] = outg[me]
@@ -379,58 +388,59 @@
         to_partner(k, t).start()
         relay(k - 1)
 
-    def expert(line, lo, dst):
-        x = xin[line, lo : lo + half].reshape(half * cap, depth)
+    def expert(lo):
+        x = xin[:, lo : lo + part].reshape(n_tp * part * cap, depth)
         g = jnp.dot(x, wg[...], preferred_element_type=f32)
         u = jnp.dot(x, wu[...], preferred_element_type=f32)
         hid = (g / (1.0 + jnp.exp(-g)) * u).astype(bf16)
-        dst[lo : lo + half] = (
-            jnp.dot(hid, wd[...], preferred_element_type=f32).astype(bf16).reshape(half, cap, depth)
+        pc[:, lo : lo + part] = (
+            jnp.dot(hid, wd[...], preferred_element_type=f32).astype(bf16).reshape(n_tp, part, cap, depth)
         )
 
     def pair_sum(k):
         c3_copy(k).wait_recv()
-        ysum[k] = (p2[k].astype(f32) + r3[k].astype(f32)).astype(bf16)
+        ysum[k] = (pc[across, k].astype(f32) + r3[k].astype(f32)).astype(bf16)
         cy_copy(k).start()
 
     def full_sum(k):
         c1_copy(k).wait_recv()
         cy_copy(k).wait_recv()
-        zsum[k] = (p0[k].astype(f32) + r1[k].astype(f32) + ry[k].astype(f32)).astype(bf16)
+        zsum[k] = (pc[t, k].astype(f32) + r1[k].astype(f32) + ry[k].astype(f32)).astype(bf16)
 
         @pl.when(k > 0)
         def _():
             cz_copy(k, me).start()
 
-    span(1, half + 1, forward)
-    for c in loads[1:]:
-        c.wait()
-    expert(t, 0, p0)
-    span(half + 1, half + 2, forward)
-    span(0, half, lambda k: to_partner(k, partner).wait_recv())
-    expert(partner, 0, p1)
-    span(0, half, lambda k: c1_copy(k).start())
-    span(half + 2, n_sp - 1, forward)
-    span(0, half, lambda k: relay_partner(k, corner).wait_recv())
-    expert(corner, 0, p3)
-    span(0, half, lambda k: c3_copy(k).start())
-    span(n_sp - 1, n_sp, forward)
-    expert(across, 0, p2)
-    span(0, half, pair_sum)
-    expert(t, half, p0)
-    relay(n_sp - 1)
-    span(half, n_sp, lambda k: to_partner(k, partner).wait_recv())
-    expert(partner, half, p1)
-    span(half, n_sp, lambda k: c1_copy(k).start())
-    span(half, n_sp, lambda k: relay_partner(k, corner).wait_recv())
-    expert(corner, half, p3)
-    span(half, n_sp, lambda k: c3_copy(k).start())
-    expert(across, half, p2)
-    span(half, n_sp, pair_sum)
-    span(0, half, full_sum)
-    span(half, n_sp, full_sum)
+    def arrive(k):
+        to_partner(k, partner).wait_recv()
+        relay_partner(k, corner).wait_recv()
+
+    def hand_over(k):
+        c3_copy(k).start()
+        c1_copy(k).start()
+
+    for step in range(7):
+        lo = step * part
+        if step < 4:
+            span(max(lo, 1), lo + part, forward)
+        if step == 4:
+            relay(n_sp - 1)
+        lo = (step - 2) * part
+        if 0 <= lo < n_sp:
+            span(lo, lo + part, pair_sum)
+        lo = (step - 3) * part
+        if 0 <= lo < n_sp:
+            span(lo, lo + part, full_sum)
+        lo = (step - 1) * part
+        if 0 <= lo < n_sp:
+            if step == 1:
+                for c in loads[1:]:
+                    c.wait()
+            span(lo, lo + part, arrive)
+            expert(lo)
+            span(lo, lo + part, hand_over)
     ret[me] = zsum[0]
-    span(1, n_sp, lambda k: cz_copy(k, peer_at(k)).wait_recv())
+    span(1, n_sp, lambda k: cz_copy(k, swap_at(k)).wait_recv())
     got = ret[...].reshape(slots, depth)
     mix = share[0] * jnp.dot(back[0], got, preferred_element_type=f32)
     for k in range(1, TOP):
@@ -506,7 +516,8 @@
             block,
             pltpu.VMEM((n_tp, n_sp, cap, depth), bf16),
         ]
-        + [block] * 10
+        + [pltpu.VMEM((n_tp, n_sp, cap, depth), bf16)]
+        + [block] * 6
         + [dma(4)]
         + [dma(n_sp)] * 6
         + [dma(n_tp)] * 2
@@ -528,8 +539,8 @@
     cap = max(2, 2 * residual.shape[0] * TOP // n_sp)
     fits = (
         n_tp == 4
-        and n_sp % 2 == 0
         and n_sp >= 8
+        and n_sp & (n_sp - 1) == 0
         and expert_gate.shape[0] == 1
         and keys.shape[1] == HEAD_DIM
         and queries.shape[0] == 128

time: 64.3 us -> 60.9 us (0.947)
  Pallas kernels: 62.5 us -> 58.6 us
    pallas_call x1, Pallas kernels: 62.5 us -> 58.6 us  [fused(): call(queries, keys.T, values.T, cum_gate.T, doc_ids.reshape(1, tok), resi...]
where the time goes in v3:
time: 60.9 us; the launch traced here: 60.3 us
  Pallas kernels  58.6 us (96%)
  other arithmetic  1.66 us (3%)
    pallas_call x1, Pallas kernels, fused(): call(queries, keys.T, values.T, cum_gate.T, doc_ids.reshape(1, tok), resi...  58.6 us
    convert_element_type x1, other arithmetic, fused(): return (base.astype(f32) + mixed).astype(bf16)  1.66 us

profile of v3, /device:TPU:0, one launch (start us, length us, event | category | flops | bytes accessed | tf_op | source)
XLA Modules:
  0.0 60.3 jit_solution(9787288486334459033)
XLA Ops:
  0.0 58.6 %shard_map.127 = (bf16[32,2048]{1,0:T(8,128)(2,1)}, f32[32,2048]{1,0:T(8,128)}) custom-call(bf16[128,256]{1,0:T(8,128)(2,1)} %q.1, bf16[64,128]{1,0:T(8,128)(2,1)} %bitcast.13, bf16[64,128]{1,0:T(8,128)(2,1)} %bitcast.14, f32[4,128]{1,0:T(4,128)} %bitcast.16, s32[1,128]{1,0:T(1,128)} %bitcast.19, bf16[32,2048]{1,0:T(8,128)(2,1)} %res.1, f32[1,2048]{1,0:T(1,128)} %bitcast.15, ...), custom_call_target="tpu_custom_call" | custom-call | tf_op jit(solution)/shard_map/pallas_call | solution.py:529
  58.6 1.7 %add_convert_fusion = bf16[32,2048]{1,0:T(8,128)(2,1)} fusion(f32[32,2048]{1,0:T(8,128)} %get-tuple-element.8, bf16[32,2048]{1,0:T(8,128)(2,1)} %get-tuple-element.7), kind=kLoop, calls=%fused_computation | loop fusion | flops 196608 | bytes 524288 | tf_op jit(solution)/shard_map/convert_element_type | solution.py:533
